TPU v7x, 128 devices: a whole 4x4x4 slice. The times are simulated.
128 devices in a mesh: fs: 16 (over z, y), tp: 4 (over x), rep: 2 (over core).
Axes of the slice: x: 4, y: 4, z: 4, core: 2. Of those that a mesh axis runs over, the one named last changes fastest.
Arguments:
- gate_grads: float32 [2, 5632, 2048], P('rep', 'fs', 'tp'), may hold values from -16 to 16, as said below
- gate_velocity: float32 [5632, 2048], P(('fs', 'rep'), 'tp'), may hold values from -31 to 31, as said below
- gate_weight: float32 [5632, 2048], P(('fs', 'rep'), 'tp'), may hold values from -4 to 4
- up_grads: float32 [2, 5632, 2048], P('rep', 'fs', 'tp'), may hold values from -16 to 16, as said below
- up_velocity: float32 [5632, 2048], P(('fs', 'rep'), 'tp'), may hold values from -31 to 31, as said below
- up_weight: float32 [5632, 2048], P(('fs', 'rep'), 'tp'), may hold values from -4 to 4
- branch_grads: float32 [2, 2048, 1024], P('rep', 'fs', 'tp'), may hold values from -16 to 16, as said below
- branch_velocity: float32 [2048, 1024], P(('fs', 'rep'), 'tp'), may hold values from -31 to 31, as said below
- branch_weight: float32 [2048, 1024], P(('fs', 'rep'), 'tp'), may hold values from -4 to 4
Outputs:
- gate_momentum: float32 [5632, 2048], P(('fs', 'rep'), 'tp')
- gate_updated: float32 [5632, 2048], P(('fs', 'rep'), 'tp')
- up_momentum: float32 [5632, 2048], P(('fs', 'rep'), 'tp')
- up_updated: float32 [5632, 2048], P(('fs', 'rep'), 'tp')
- branch_momentum: float32 [2048, 1024], P(('fs', 'rep'), 'tp')
- branch_updated: float32 [2048, 1024], P(('fs', 'rep'), 'tp')
Inputs may be any that keep to these rules, and one draw needn't show every extreme that they name: `gate_grads`: entries vary in scale over rows and over columns. `up_grads`: entries vary in scale over rows and over columns. `branch_grads`: entries vary in scale over rows and over columns. `gate_velocity`: entries vary in scale over rows and over columns. `up_velocity`: entries vary in scale over rows and over columns. `branch_velocity`: entries vary in scale over rows and over columns.
All inputs are finite; a program needn't handle non-finite values.
Results may differ from a plain program's by a relative error of at most 0.039.
Values may be sent and summed in bfloat16 or wider, within the bound.
A program may use at most 64 MiB of HBM per device.

v0:
```python
import math
import jax
import jax.numpy as jnp
from jax import lax
from jax.sharding import Mesh
from jax.sharding import PartitionSpec as P

D = 2048
FF = 5632
ITERS = 3
FS_REP = ("fs_0", "fs_1", "rep")
FS_TP_REP = ("fs_0", "fs_1", "tp", "rep")
FS = ("fs_0", "fs_1")
MOMENT = 0.95
COEF_ONE = 3.4445
COEF_THREE = -4.775
COEF_FIVE = 2.0315
SAFETY = 2.0
RATE = 0.5
SHRINK = 0.95


def joined_along(tiles, dim):
    lengths = list(tiles.shape[1:])
    lengths[dim] *= tiles.shape[0]
    return jnp.moveaxis(tiles, 0, dim).reshape(lengths)


def from_everyone(value, axis):
    devices = lax.axis_size(axis)
    return lax.all_to_all(
        jnp.broadcast_to(value[None], (devices, *value.shape)), axis, 0, 0, tiled=True
    )


def gathered_copies(value, axis, dim):
    return joined_along(from_everyone(value, axis), dim)


def split_up(value, dim, devices):
    before, after = (value.shape[:dim], value.shape[dim + 1 :])
    return jnp.moveaxis(value.reshape(*before, devices, -1, *after), dim, 0)


def sum_at_owner(value, axis, dim):
    devices = lax.axis_size(axis)
    tiles = lax.all_to_all(split_up(value, dim, devices), axis, 0, 0, tiled=True)
    return jnp.sum(tiles.astype(jnp.float32), axis=0)


def by_axis(value, axes):
    for axis in axes:
        value = lax.psum(value, axis)
    return value


def side_by_side(arrays, axis, dim, along):
    ends, at = ([], 0)
    for a in arrays[:-1]:
        at += a.shape[along]
        ends.append(at)
    both = jnp.concatenate(arrays, axis=along)
    return tuple(jnp.split(sum_at_owner(both, axis, dim), ends, axis=along))


def rounded(part):
    narrow = lax.optimization_barrier(part.astype(jnp.bfloat16))
    return narrow.astype(jnp.float32)


def gram(current):
    whole = gathered_copies(current, "tp", 1)
    part = lax.dot_general(
        whole, current, (((0,), (0,)), ((), ())), preferred_element_type=jnp.float32
    )
    share = sum_at_owner(rounded(part).astype(jnp.bfloat16), FS_REP, 0)
    return (whole, share)


def spread(share):
    return lax.all_gather(share, FS_REP, axis=0, tiled=True)


def second_product(ymat, columns):
    return jnp.dot(gathered_copies(ymat, "tp", 1), columns, preferred_element_type=jnp.float32)


def combine(current, ymat, zmat, factor):
    mixed = COEF_ONE * factor * current.astype(jnp.float32) + COEF_THREE * ymat.astype(jnp.float32)
    return (mixed + COEF_FIVE * zmat.astype(jnp.float32)).astype(jnp.bfloat16)


def orthogonalize(starts):
    firsts = [gram(current) for current in starts]
    squares = tuple((jnp.sum(jnp.square(current.astype(jnp.float32))) for current in starts))
    seconds = tuple((jnp.sum(share * share) for whole, share in firsts))
    totals = jax.tree.map(lambda part: by_axis(part, FS_TP_REP), squares + seconds)
    first_sums, gram_sums = (totals[:3], totals[3:])
    finals = []
    for current, pair, first_sum, gram_sum in zip(starts, firsts, first_sums, gram_sums):
        whole, share = pair
        ratio = SAFETY * (gram_sum + 1.0) / (first_sum + 1.0)
        factor = lax.rsqrt(ratio)
        columns = spread((share / ratio).astype(jnp.bfloat16))
        ymat = (jnp.dot(whole, columns, preferred_element_type=jnp.float32) * factor).astype(
            jnp.bfloat16
        )
        zmat = second_product(ymat, columns).astype(jnp.bfloat16)
        current = combine(current, ymat, zmat, factor)
        for index in range(ITERS - 1):
            whole, share = gram(current)
            columns = spread(share.astype(jnp.bfloat16))
            ymat = jnp.dot(whole, columns, preferred_element_type=jnp.float32).astype(jnp.bfloat16)
            zmat = second_product(ymat, columns).astype(jnp.bfloat16)
            current = combine(current, ymat, zmat, 1.0)
        finals.append(current)
    return tuple(finals)


def local(
    gate_grads,
    gate_velocity,
    gate_weight,
    up_grads,
    up_velocity,
    up_weight,
    branch_grads,
    branch_velocity,
    branch_weight,
):
    totals = (
        *side_by_side(
            (gate_grads.astype(jnp.bfloat16), up_grads.astype(jnp.bfloat16)), "rep", 1, 0
        ),
        sum_at_owner(branch_grads.astype(jnp.bfloat16), "rep", 1),
    )
    velocities = (gate_velocity, up_velocity, branch_velocity)
    moments = [MOMENT * velocity + total[0] for velocity, total in zip(velocities, totals)]
    starts = tuple((moment.astype(jnp.bfloat16) for moment in moments))
    finals = orthogonalize(starts)
    weights = (gate_weight, up_weight, branch_weight)
    heights = (FF, FF, D)
    results = []
    for moment, weight, final, height in zip(moments, weights, finals, heights):
        results.append(moment)
        results.append(SHRINK * weight - RATE * math.sqrt(height) * final.astype(jnp.float32))
    return tuple(results)


def solution(mesh):
    torus = Mesh(
        mesh.devices.reshape(4, 4, mesh.shape["tp"], mesh.shape["rep"]),
        ("fs_0", "fs_1", "tp", "rep"),
    )
    return jax.shard_map(
        local,
        mesh=torus,
        in_specs=(
            P("rep", FS, "tp"),
            P(FS_REP, "tp"),
            P(FS_REP, "tp"),
            P("rep", FS, "tp"),
            P(FS_REP, "tp"),
            P(FS_REP, "tp"),
            P("rep", FS, "tp"),
            P(FS_REP, "tp"),
            P(FS_REP, "tp"),
        ),
        out_specs=(
            P(FS_REP, "tp"),
            P(FS_REP, "tp"),
            P(FS_REP, "tp"),
            P(FS_REP, "tp"),
            P(FS_REP, "tp"),
            P(FS_REP, "tp"),
        ),
        check_vma=False,
    )
```

profile of v0, /device:TPU:0, one launch (start us, length us, event | category | flops | bytes accessed | tf_op | source)
XLA Modules:
  0.0 692.4 jit_solution(9970207772940206711)
XLA Ops:
  32.0 13.1 %all_to_all.145 = bf16[4,176,512]{2,1,0:T(8,128)(2,1)S(1)} all-to-all(bf16[4,176,512]{2,1,0:T(8,128)(2,1)S(1)} %broadcast_in_dim.42), channel_id=1, replica_groups=mesh['fs_0'=4,'fs_1'=4,'tp'=4,'rep'=2] {'tp'}, dimensions={0} | all-to-all | bytes 1441792 | tf_op jit(solution)/shard_map/all_to_all | solution.py:31
  50.7 8.4 %all-to-all-done.1 = bf16[4,176,512]{2,1,0:T(8,128)(2,1)S(1)} async-done(((bf16[4,176,512]{2,1,0:T(8,128)(2,1)}), bf16[4,176,512]{2,1,0:T(8,128)(2,1)S(1)}, u32[]{:S(2)}, u32[]{:S(2)}) %all-to-all-start.1) | async-done | bytes 720928 | tf_op jit(solution)/shard_map/all_to_all | solution.py:31
  59.1 8.3 %all-to-all-start.21 = ((bf16[32,32,256]{2,1,0:T(8,128)(2,1)}), bf16[32,32,256]{2,1,0:T(8,128)(2,1)S(1)}, u32[]{:S(2)}, u32[]{:S(2)}) async-start(bf16[32,32,256]{2,1,0:T(8,128)(2,1)} %bitcast.24), calls=%async_computation.21 | async-start | bytes 1048576 | tf_op jit(solution)/shard_map/all_to_all | solution.py:47
  69.5 9.5 %all-to-all-done.21 = bf16[32,32,256]{2,1,0:T(8,128)(2,1)S(1)} async-done(((bf16[32,32,256]{2,1,0:T(8,128)(2,1)}), bf16[32,32,256]{2,1,0:T(8,128)(2,1)S(1)}, u32[]{:S(2)}, u32[]{:S(2)}) %all-to-all-start.21) | async-done | bytes 524320 | tf_op jit(solution)/shard_map/all_to_all | solution.py:47
  88.0 25.9 %all-to-all-done.11 = bf16[32,64,512]{2,1,0:T(8,128)(2,1)S(1)} async-done(((bf16[32,64,512]{2,1,0:T(8,128)(2,1)}), bf16[32,64,512]{2,1,0:T(8,128)(2,1)S(1)}, u32[]{:S(2)}, u32[]{:S(2)}) %all-to-all-start.11) | async-done | bytes 2097184 | tf_op jit(solution)/shard_map/all_to_all | solution.py:47
  122.7 26.0 %all-to-all-done.2 = bf16[32,64,512]{2,1,0:T(8,128)(2,1)} async-done(((bf16[32,64,512]{2,1,0:T(8,128)(2,1)}), bf16[32,64,512]{2,1,0:T(8,128)(2,1)}, u32[]{:S(2)}, u32[]{:S(2)}) %all-to-all-start.2) | async-done | bytes 2097184 | tf_op jit(solution)/shard_map/all_to_all | solution.py:47
  151.4 8.4 %all-reduce.2 = (f32[]{:T(128)}, f32[]{:T(128)}, f32[]{:T(128)}, f32[]{:T(128)}, f32[]{:T(128)}, /*index=5*/f32[]{:T(128)}) all-reduce(f32[]{:T(128)} %multiply_reduce_fusion.1, f32[]{:T(128)} %get-tuple-element.39, f32[]{:T(128)} %multiply_reduce_fusion, ...), channel_id=1, replica_groups=mesh['fs_0'=4,'fs_1'=4,'tp'=4,'rep'=2] {'fs_0'}, use_global_device_ids=true, to_apply=%region_3.0 | all-reduce | flops 6 | bytes 48 | tf_op jit(solution)/shard_map/psum | solution.py:53
  159.8 9.6 %all-reduce.1 = (f32[]{:T(128)}, f32[]{:T(128)}, f32[]{:T(128)}, f32[]{:T(128)}, f32[]{:T(128)}, /*index=5*/f32[]{:T(128)}) all-reduce(f32[]{:T(128)} %get-tuple-element.18, f32[]{:T(128)} %get-tuple-element.19, f32[]{:T(128)} %get-tuple-element.20, f32[]{:T(128)} %get-tuple-element.21, ...), channel_id=1, replica_groups=mesh['fs_0'=4,'fs_1'=4,'tp'=4,'rep'=2] {'fs_1'}, use_global_device_ids=true, to_apply=%region_4.0 | all-reduce | flops 6 | bytes 48 | tf_op jit(solution)/shard_map/psum | solution.py:53
  169.4 9.6 %all-reduce = (f32[]{:T(128)}, f32[]{:T(128)}, f32[]{:T(128)}, f32[]{:T(128)}, f32[]{:T(128)}, /*index=5*/f32[]{:T(128)}) all-reduce(f32[]{:T(128)} %get-tuple-element.12, f32[]{:T(128)} %get-tuple-element.13, f32[]{:T(128)} %get-tuple-element.14, f32[]{:T(128)} %get-tuple-element.15, ...), channel_id=1, replica_groups=mesh['fs_0'=4,'fs_1'=4,'tp'=4,'rep'=2] {'tp'}, use_global_device_ids=true, to_apply=%region_5.0 | all-reduce | flops 6 | bytes 48 | tf_op jit(solution)/shard_map/psum | solution.py:53
  186.1 37.8 %all-gather.13.cloned.1.call-done = bf16[2048,512]{1,0:T(8,128)(2,1)} async-done(((bf16[64,512]{1,0:T(8,128)(2,1)}), bf16[2048,512]{1,0:T(8,128)(2,1)}) %all-gather.13.cloned.1.call-update) | async-done | bytes 2097168 | tf_op jit(solution)/shard_map/all_gather | solution.py:81
  231.2 12.0 %all-to-all-done.12 = bf16[4,176,512]{2,1,0:T(8,128)(2,1)S(1)} async-done(((bf16[4,176,512]{2,1,0:T(8,128)(2,1)}), bf16[4,176,512]{2,1,0:T(8,128)(2,1)S(1)}, u32[]{:S(2)}, u32[]{:S(2)}) %all-to-all-start.12) | async-done | bytes 720928 | tf_op jit(solution)/shard_map/all_to_all | solution.py:31
  245.5 13.5 %all_to_all.146 = bf16[4,176,512]{2,1,0:T(8,128)(2,1)S(1)} all-to-all(bf16[4,176,512]{2,1,0:T(8,128)(2,1)S(1)} %broadcast_in_dim.44), channel_id=1, replica_groups=mesh['fs_0'=4,'fs_1'=4,'tp'=4,'rep'=2] {'tp'}, dimensions={0} | all-to-all | bytes 1441792 | tf_op jit(solution)/shard_map/all_to_all | solution.py:31
  259.8 33.5 %all_to_all.147 = bf16[32,64,512]{2,1,0:T(8,128)(2,1)S(1)} all-to-all(bf16[32,64,512]{2,1,0:T(8,128)(2,1)S(1)} %bitcast.134), channel_id=1, replica_groups=mesh['fs_0'=4,'fs_1'=4,'tp'=4,'rep'=2] {'fs_0','fs_1','rep'}, dimensions={0} | all-to-all | bytes 4194304 | tf_op jit(solution)/shard_map/all_to_all | solution.py:47
  301.6 12.0 %all-to-all-done.3 = bf16[4,176,512]{2,1,0:T(8,128)(2,1)S(1)} async-done(((bf16[4,176,512]{2,1,0:T(8,128)(2,1)}), bf16[4,176,512]{2,1,0:T(8,128)(2,1)S(1)}, u32[]{:S(2)}, u32[]{:S(2)}) %all-to-all-start.3) | async-done | bytes 720928 | tf_op jit(solution)/shard_map/all_to_all | solution.py:31
  315.4 13.7 %all_to_all.148 = bf16[4,176,512]{2,1,0:T(8,128)(2,1)S(1)} all-to-all(bf16[4,176,512]{2,1,0:T(8,128)(2,1)S(1)} %broadcast_in_dim.38), channel_id=1, replica_groups=mesh['fs_0'=4,'fs_1'=4,'tp'=4,'rep'=2] {'tp'}, dimensions={0} | all-to-all | bytes 1441792 | tf_op jit(solution)/shard_map/all_to_all | solution.py:31
  330.0 32.8 %all_to_all.149 = bf16[32,64,512]{2,1,0:T(8,128)(2,1)S(1)} all-to-all(bf16[32,64,512]{2,1,0:T(8,128)(2,1)S(1)} %bitcast.135), channel_id=1, replica_groups=mesh['fs_0'=4,'fs_1'=4,'tp'=4,'rep'=2] {'fs_0','fs_1','rep'}, dimensions={0} | all-to-all | bytes 4194304 | tf_op jit(solution)/shard_map/all_to_all | solution.py:47
  366.3 14.7 %all_to_all.150 = bf16[4,176,512]{2,1,0:T(8,128)(2,1)S(1)} all-to-all(bf16[4,176,512]{2,1,0:T(8,128)(2,1)S(1)} %broadcast_in_dim.45), channel_id=1, replica_groups=mesh['fs_0'=4,'fs_1'=4,'tp'=4,'rep'=2] {'tp'}, dimensions={0} | all-to-all | bytes 1441792 | tf_op jit(solution)/shard_map/all_to_all | solution.py:31
  381.6 13.4 %all_to_all.151 = bf16[4,176,512]{2,1,0:T(8,128)(2,1)S(1)} all-to-all(bf16[4,176,512]{2,1,0:T(8,128)(2,1)S(1)} %broadcast_in_dim.46), channel_id=1, replica_groups=mesh['fs_0'=4,'fs_1'=4,'tp'=4,'rep'=2] {'tp'}, dimensions={0} | all-to-all | bytes 1441792 | tf_op jit(solution)/shard_map/all_to_all | solution.py:31
  395.9 33.2 %all_to_all.152 = bf16[32,64,512]{2,1,0:T(8,128)(2,1)S(1)} all-to-all(bf16[32,64,512]{2,1,0:T(8,128)(2,1)S(1)} %bitcast.136), channel_id=1, replica_groups=mesh['fs_0'=4,'fs_1'=4,'tp'=4,'rep'=2] {'fs_0','fs_1','rep'}, dimensions={0} | all-to-all | bytes 4194304 | tf_op jit(solution)/shard_map/all_to_all | solution.py:47
  432.5 14.7 %all_to_all.153 = bf16[4,176,512]{2,1,0:T(8,128)(2,1)S(1)} all-to-all(bf16[4,176,512]{2,1,0:T(8,128)(2,1)S(1)} %broadcast_in_dim.39), channel_id=1, replica_groups=mesh['fs_0'=4,'fs_1'=4,'tp'=4,'rep'=2] {'tp'}, dimensions={0} | all-to-all | bytes 1441792 | tf_op jit(solution)/shard_map/all_to_all | solution.py:31
  447.9 13.4 %all_to_all.154 = bf16[4,176,512]{2,1,0:T(8,128)(2,1)S(1)} all-to-all(bf16[4,176,512]{2,1,0:T(8,128)(2,1)S(1)} %broadcast_in_dim.40), channel_id=1, replica_groups=mesh['fs_0'=4,'fs_1'=4,'tp'=4,'rep'=2] {'tp'}, dimensions={0} | all-to-all | bytes 1441792 | tf_op jit(solution)/shard_map/all_to_all | solution.py:31
  469.8 28.7 %all-to-all-done.8 = bf16[32,64,512]{2,1,0:T(8,128)(2,1)S(1)} async-done(((bf16[32,64,512]{2,1,0:T(8,128)(2,1)}), bf16[32,64,512]{2,1,0:T(8,128)(2,1)S(1)}, u32[]{:S(2)}, u32[]{:S(2)}) %all-to-all-start.8) | async-done | bytes 2097184 | tf_op jit(solution)/shard_map/all_to_all | solution.py:47
  500.2 21.8 %all_gather.33 = bf16[1024,256]{1,0:T(8,128)(2,1)S(1)} all-gather(bf16[32,256]{1,0:T(8,128)(2,1)S(1)} %divide_convert_fusion.2), channel_id=1, replica_groups=mesh['fs_0'=4,'fs_1'=4,'tp'=4,'rep'=2] {'fs_0','fs_1','rep'}, dimensions={0}, use_global_device_ids=true | all-gather | bytes 540672 | tf_op jit(solution)/shard_map/all_gather | solution.py:81
  527.1 6.0 all-to-all-done.22
  534.1 8.4 %all_to_all.155 = bf16[4,64,256]{2,1,0:T(8,128)(2,1)S(1)} all-to-all(bf16[4,64,256]{2,1,0:T(8,128)(2,1)S(1)} %broadcast_in_dim.50), channel_id=1, replica_groups=mesh['fs_0'=4,'fs_1'=4,'tp'=4,'rep'=2] {'tp'}, dimensions={0} | all-to-all | bytes 262144 | tf_op jit(solution)/shard_map/all_to_all | solution.py:31
  542.8 17.2 %all_to_all.156 = bf16[32,32,256]{2,1,0:T(8,128)(2,1)S(1)} all-to-all(bf16[32,32,256]{2,1,0:T(8,128)(2,1)S(1)} %bitcast.164), channel_id=1, replica_groups=mesh['fs_0'=4,'fs_1'=4,'tp'=4,'rep'=2] {'fs_0','fs_1','rep'}, dimensions={0} | all-to-all | bytes 1048576 | tf_op jit(solution)/shard_map/all_to_all | solution.py:47
  560.1 22.5 %all_gather.34 = bf16[1024,256]{1,0:T(8,128)(2,1)S(1)} all-gather(bf16[32,256]{1,0:T(8,128)(2,1)S(1)} %reduce_sum.186), channel_id=1, replica_groups=mesh['fs_0'=4,'fs_1'=4,'tp'=4,'rep'=2] {'fs_0','fs_1','rep'}, dimensions={0}, use_global_device_ids=true | all-gather | bytes 540672 | tf_op jit(solution)/shard_map/all_gather | solution.py:81
  582.9 8.4 %all_to_all.157 = bf16[4,64,256]{2,1,0:T(8,128)(2,1)S(1)} all-to-all(bf16[4,64,256]{2,1,0:T(8,128)(2,1)S(1)} %broadcast_in_dim.51), channel_id=1, replica_groups=mesh['fs_0'=4,'fs_1'=4,'tp'=4,'rep'=2] {'tp'}, dimensions={0} | all-to-all | bytes 262144 | tf_op jit(solution)/shard_map/all_to_all | solution.py:31
  591.6 8.4 %all_to_all.158 = bf16[4,64,256]{2,1,0:T(8,128)(2,1)S(1)} all-to-all(bf16[4,64,256]{2,1,0:T(8,128)(2,1)S(1)} %broadcast_in_dim.52), channel_id=1, replica_groups=mesh['fs_0'=4,'fs_1'=4,'tp'=4,'rep'=2] {'tp'}, dimensions={0} | all-to-all | bytes 262144 | tf_op jit(solution)/shard_map/all_to_all | solution.py:31
  600.3 16.4 %all_to_all.159 = bf16[32,32,256]{2,1,0:T(8,128)(2,1)S(1)} all-to-all(bf16[32,32,256]{2,1,0:T(8,128)(2,1)S(1)} %bitcast.165), channel_id=1, replica_groups=mesh['fs_0'=4,'fs_1'=4,'tp'=4,'rep'=2] {'fs_0','fs_1','rep'}, dimensions={0} | all-to-all | bytes 1048576 | tf_op jit(solution)/shard_map/all_to_all | solution.py:47
  616.8 22.8 %all_gather.35 = bf16[1024,256]{1,0:T(8,128)(2,1)S(1)} all-gather(bf16[32,256]{1,0:T(8,128)(2,1)S(1)} %reduce_sum.187), channel_id=1, replica_groups=mesh['fs_0'=4,'fs_1'=4,'tp'=4,'rep'=2] {'fs_0','fs_1','rep'}, dimensions={0}, use_global_device_ids=true | all-gather | bytes 540672 | tf_op jit(solution)/shard_map/all_gather | solution.py:81
  657.3 9.0 %all-to-all-done.18 = bf16[4,176,512]{2,1,0:T(8,128)(2,1)S(1)} async-done(((bf16[4,176,512]{2,1,0:T(8,128)(2,1)}), bf16[4,176,512]{2,1,0:T(8,128)(2,1)S(1)}, u32[]{:S(2)}, u32[]{:S(2)}) %all-to-all-start.18) | async-done | bytes 720928 | tf_op jit(solution)/shard_map/all_to_all | solution.py:31
  (203 shorter events, 140.5 us)
Async XLA Ops:
  8.7 6.6 all-to-all-start.19
  15.3 5.5 all-to-all-start
  20.3 29.3 %copy-start.31 = (bf16[64,256]{1,0:T(8,128)(2,1)}, bf16[64,256]{1,0:T(8,128)(2,1)S(1)}, u32[]{:S(2)}) copy-start(bf16[64,256]{1,0:T(8,128)(2,1)S(1)} %get-tuple-element.31) | copy-start | bytes 98308
  21.5 10.4 %all-to-all-start.20 = ((bf16[4,64,256]{2,1,0:T(8,128)(2,1)}), bf16[4,64,256]{2,1,0:T(8,128)(2,1)S(1)}, u32[]{:S(2)}, u32[]{:S(2)}) async-start(bf16[4,64,256]{2,1,0:T(8,128)(2,1)} %broadcast_in_dim.48), calls=%async_computation.20 | async-start | bytes 262144 | tf_op jit(solution)/shard_map/all_to_all | solution.py:31
  27.7 18.3 %copy-start.12 = (bf16[176,512]{1,0:T(8,128)(2,1)}, bf16[176,512]{1,0:T(8,128)(2,1)S(1)}, u32[]{:S(2)}) copy-start(bf16[176,512]{1,0:T(8,128)(2,1)S(1)} %get-tuple-element.40) | copy-start | bytes 540676
  27.7 39.8 %copy-start.13 = (bf16[176,512]{1,0:T(8,128)(2,1)}, bf16[176,512]{1,0:T(8,128)(2,1)S(1)}, u32[]{:S(2)}) copy-start(bf16[176,512]{1,0:T(8,128)(2,1)S(1)} %get-tuple-element.34) | copy-start | bytes 540676
  46.0 13.0 %all-to-all-start.1 = ((bf16[4,176,512]{2,1,0:T(8,128)(2,1)}), bf16[4,176,512]{2,1,0:T(8,128)(2,1)S(1)}, u32[]{:S(2)}, u32[]{:S(2)}) async-start(bf16[4,176,512]{2,1,0:T(8,128)(2,1)} %broadcast_in_dim.36), calls=%async_computation.1 | async-start | bytes 1441792 | tf_op jit(solution)/shard_map/all_to_all | solution.py:31
  59.1 19.9 %all-to-all-start.21 = ((bf16[32,32,256]{2,1,0:T(8,128)(2,1)}), bf16[32,32,256]{2,1,0:T(8,128)(2,1)S(1)}, u32[]{:S(2)}, u32[]{:S(2)}) async-start(bf16[32,32,256]{2,1,0:T(8,128)(2,1)} %bitcast.24), calls=%async_computation.21 | async-start | bytes 1048576 | tf_op jit(solution)/shard_map/all_to_all | solution.py:47
  79.8 34.1 %all-to-all-start.11 = ((bf16[32,64,512]{2,1,0:T(8,128)(2,1)}), bf16[32,64,512]{2,1,0:T(8,128)(2,1)S(1)}, u32[]{:S(2)}, u32[]{:S(2)}) async-start(bf16[32,64,512]{2,1,0:T(8,128)(2,1)} %bitcast.133), calls=%async_computation.11 | async-start | bytes 4194304 | tf_op jit(solution)/shard_map/all_to_all | solution.py:47
  113.9 34.8 %all-to-all-start.2 = ((bf16[32,64,512]{2,1,0:T(8,128)(2,1)}), bf16[32,64,512]{2,1,0:T(8,128)(2,1)}, u32[]{:S(2)}, u32[]{:S(2)}) async-start(bf16[32,64,512]{2,1,0:T(8,128)(2,1)} %bitcast.132), calls=%async_computation.2 | async-start | bytes 4194304 | tf_op jit(solution)/shard_map/all_to_all | solution.py:47
  118.7 105.2 %all-gather.13.cloned.1.call-start = ((), (), s32[]{:S(2)}) async-start(), calls=%async_computation.32 | async-start | bytes 2162688 | tf_op jit(solution)/shard_map/all_gather | solution.py:81
  122.7 60.7 %copy-start.23 = (f32[64,512]{1,0:T(8,128)S(1)}, f32[64,512]{1,0:T(8,128)}, u32[]{:S(2)}) copy-start(f32[64,512]{1,0:T(8,128)} %copy-done.22) | copy-start | bytes 393220
  184.1 110.2 %all-gather.7.cloned.1.call-start = ((), (), s32[]{:S(2)}) async-start(), calls=%async_computation.29 | async-start | bytes 2162688 | tf_op jit(solution)/shard_map/all_gather | solution.py:81
  226.0 17.2 %copy-start.14 = (bf16[176,512]{1,0:T(8,128)(2,1)S(1)}, bf16[176,512]{1,0:T(8,128)(2,1)}, u32[]{:S(2)}) copy-start(bf16[176,512]{1,0:T(8,128)(2,1)} %copy-done.13) | copy-start | bytes 540676
  226.9 16.2 %all-to-all-start.12 = ((bf16[4,176,512]{2,1,0:T(8,128)(2,1)}), bf16[4,176,512]{2,1,0:T(8,128)(2,1)S(1)}, u32[]{:S(2)}, u32[]{:S(2)}) async-start(bf16[4,176,512]{2,1,0:T(8,128)(2,1)} %broadcast_in_dim.43), calls=%async_computation.12 | async-start | bytes 1441792 | tf_op jit(solution)/shard_map/all_to_all | solution.py:31
  231.2 132.8 %all-gather.15.cloned.1.call-start = ((), (), s32[]{:S(2)}) async-start(), calls=%async_computation.33 | async-start | bytes 2162688 | tf_op jit(solution)/shard_map/all_gather | solution.py:81
  297.2 16.6 %copy-start.8 = (bf16[2048,512]{1,0:T(8,128)(2,1)S(1)}, bf16[2048,512]{1,0:T(8,128)(2,1)}, u32[]{:S(2)}) copy-start(bf16[2048,512]{1,0:T(8,128)(2,1)} %all-gather.7.cloned.1.call-done) | copy-start | bytes 6291460
  298.1 15.6 %all-to-all-start.3 = ((bf16[4,176,512]{2,1,0:T(8,128)(2,1)}), bf16[4,176,512]{2,1,0:T(8,128)(2,1)S(1)}, u32[]{:S(2)}, u32[]{:S(2)}) async-start(bf16[4,176,512]{2,1,0:T(8,128)(2,1)} %broadcast_in_dim.37), calls=%async_computation.3 | async-start | bytes 1441792 | tf_op jit(solution)/shard_map/all_to_all | solution.py:31
  301.6 128.5 %all-gather.9.cloned.1.call-start = ((), (), s32[]{:S(2)}) async-start(), calls=%async_computation.30 | async-start | bytes 2162688 | tf_op jit(solution)/shard_map/all_gather | solution.py:81
  363.8 280.9 %all-gather.17.cloned.1.call-start = ((), (), s32[]{:S(2)}) async-start(), calls=%async_computation.34 | async-start | bytes 2162688 | tf_op jit(solution)/shard_map/all_gather | solution.py:81
  366.2 14.8 %copy-start.9 = (bf16[2048,512]{1,0:T(8,128)(2,1)S(1)}, bf16[2048,512]{1,0:T(8,128)(2,1)}, u32[]{:S(2)}) copy-start(bf16[2048,512]{1,0:T(8,128)(2,1)} %all-gather.15.cloned.1.call-done) | copy-start | bytes 6291460
  432.4 14.8 %copy-start.10 = (bf16[2048,512]{1,0:T(8,128)(2,1)S(1)}, bf16[2048,512]{1,0:T(8,128)(2,1)}, u32[]{:S(2)}) copy-start(bf16[2048,512]{1,0:T(8,128)(2,1)} %all-gather.9.cloned.1.call-done) | copy-start | bytes 6291460
  432.4 14.8 %copy-start.28 = (bf16[176,512]{1,0:T(8,128)(2,1)S(1)}, bf16[176,512]{1,0:T(8,128)(2,1)}, u32[]{:S(2)}) copy-start(bf16[176,512]{1,0:T(8,128)(2,1)} %copy-done.27) | copy-start | bytes 540676
  447.8 15.6 %copy-start.17 = (bf16[176,512]{1,0:T(8,128)(2,1)}, bf16[176,512]{1,0:T(8,128)(2,1)S(1)}, u32[]{:S(2)}) copy-start(bf16[176,512]{1,0:T(8,128)(2,1)S(1)} %fusion.21) | copy-start | bytes 540676
  463.4 35.1 %all-to-all-start.8 = ((bf16[32,64,512]{2,1,0:T(8,128)(2,1)}), bf16[32,64,512]{2,1,0:T(8,128)(2,1)S(1)}, u32[]{:S(2)}, u32[]{:S(2)}) async-start(bf16[32,64,512]{2,1,0:T(8,128)(2,1)} %bitcast.131), calls=%async_computation.8 | async-start | bytes 4194304 | tf_op jit(solution)/shard_map/all_to_all | solution.py:47
  468.4 186.7 %all-gather.11.cloned.1.call-start = ((), (), s32[]{:S(2)}) async-start(), calls=%async_computation.31 | async-start | bytes 2162688 | tf_op jit(solution)/shard_map/all_gather | solution.py:81
  523.8 9.4 %all-to-all-start.22 = ((bf16[4,64,256]{2,1,0:T(8,128)(2,1)}), bf16[4,64,256]{2,1,0:T(8,128)(2,1)S(1)}, u32[]{:S(2)}, u32[]{:S(2)}) async-start(bf16[4,64,256]{2,1,0:T(8,128)(2,1)} %broadcast_in_dim.49), calls=%async_computation.22 | async-start | bytes 262144 | tf_op jit(solution)/shard_map/all_to_all | solution.py:31
  591.6 49.0 %copy-start.32 = (bf16[64,256]{1,0:T(8,128)(2,1)}, bf16[64,256]{1,0:T(8,128)(2,1)S(1)}, u32[]{:S(2)}) copy-start(bf16[64,256]{1,0:T(8,128)(2,1)S(1)} %fusion.43) | copy-start | bytes 98308
  641.3 9.4 %all-to-all-start.28 = ((bf16[4,64,256]{2,1,0:T(8,128)(2,1)}), bf16[4,64,256]{2,1,0:T(8,128)(2,1)S(1)}, u32[]{:S(2)}, u32[]{:S(2)}) async-start(bf16[4,64,256]{2,1,0:T(8,128)(2,1)} %broadcast_in_dim.53), calls=%async_computation.28 | async-start | bytes 262144 | tf_op jit(solution)/shard_map/all_to_all | solution.py:31
  651.6 14.7 %all-to-all-start.18 = ((bf16[4,176,512]{2,1,0:T(8,128)(2,1)}), bf16[4,176,512]{2,1,0:T(8,128)(2,1)S(1)}, u32[]{:S(2)}, u32[]{:S(2)}) async-start(bf16[4,176,512]{2,1,0:T(8,128)(2,1)} %broadcast_in_dim.47), calls=%async_computation.18 | async-start | bytes 1441792 | tf_op jit(solution)/shard_map/all_to_all | solution.py:31
  655.1 16.9 %copy-start.5 = (bf16[1024,256]{1,0:T(8,128)(2,1)S(1)}, bf16[1024,256]{1,0:T(8,128)(2,1)}, u32[]{:S(2)}) copy-start(bf16[1024,256]{1,0:T(8,128)(2,1)} %copy-done.4) | copy-start | bytes 1572868
  667.4 13.9 %all-to-all-start.9 = ((bf16[4,176,512]{2,1,0:T(8,128)(2,1)}), bf16[4,176,512]{2,1,0:T(8,128)(2,1)S(1)}, u32[]{:S(2)}, u32[]{:S(2)}) async-start(bf16[4,176,512]{2,1,0:T(8,128)(2,1)} %broadcast_in_dim.41), calls=%async_computation.9 | async-start | bytes 1441792 | tf_op jit(solution)/shard_map/all_to_all | solution.py:31
  (28 other events, 184.6 us)
Sparse Core Ops, SparseCore 0:
  184.2 39.6 all-gather.12
  226.7 42.9 all-gather.6
  294.4 39.9 all-gather.14
  363.9 39.6 all-gather.8
  430.2 39.6 all-gather.16
  499.5 39.2 all-gather.10
where the time goes:
time: 695 us; the launch traced here: 692 us
  blocking collectives  353 us (51%)
  waiting for transfers between devices  189 us (27%)
  starting transfers between devices  58.7 us (8%)
  matrix products  37.4 us (5%)
  between operations  19 us (3%)
  other arithmetic  18.2 us (3%)
  local copies, waits for them, and re-layouts  17.1 us (2%)
    all_to_all x5, blocking collectives, sum_at_owner(): lax.all_to_all(split_up(value, dim, devices), axis, 0, 0, tiled=True)  133 us
    all_to_all x10, blocking collectives, from_everyone(): lax.all_to_all(jnp.broadcast_to(value[None], (devices, *value.shape)), ax...  122 us
    all_to_all x6, waiting for transfers between devices, sum_at_owner(): lax.all_to_all(split_up(value, dim, devices), axis, 0, 0, tiled=True)  90.6 us
    all_gather x3, blocking collectives, spread(): return lax.all_gather(share, FS_REP, axis=0, tiled=True)  67.1 us
    all_to_all x8, waiting for transfers between devices, from_everyone(): lax.all_to_all(jnp.broadcast_to(value[None], (devices, *value.shape)), ax...  60.8 us
    all_gather x6, waiting for transfers between devices, spread(): return lax.all_gather(share, FS_REP, axis=0, tiled=True)  37.9 us
    psum x4, blocking collectives, by_axis(): value = lax.psum(value, axis)  30.8 us
    all_to_all x8, starting transfers between devices, from_everyone(): lax.all_to_all(jnp.broadcast_to(value[None], (devices, *value.shape)), ax...  29.3 us
  transfers between devices with their start and end apart: 20, of which 14 were waited for; matrix products, arithmetic and copies ran while one was open for 8% of the time, Pallas kernels for 0%

commit v1 on v0

--- a/solution.py
+++ b/solution.py
@@ -78,7 +78,9 @@
 
 
 def spread(share):
-    return lax.all_gather(share, FS_REP, axis=0, tiled=True)
+    return jnp.concatenate(
+        lax.all_to_all(jnp.stack([share] * lax.axis_size(FS_REP)), FS_REP, 0, 0), axis=0
+    )
 
 
 def second_product(ymat, columns):

time: 695 us -> 837 us (1.20)
  waiting for transfers between devices: 189 us -> 475 us
  blocking collectives: 353 us -> 82.4 us
  starting transfers between devices: 58.7 us -> 144 us
  local copies, waits for them, and re-layouts: 17.1 us -> 53.5 us
  between operations: 19 us -> 5.61 us
  matrix products: 37.4 us -> 46.4 us
    all_to_all x0 -> x8, waiting for transfers between devices: none -> 186 us  [spread(): lax.all_to_all(jnp.stack([share] * lax.axis_size(FS_REP)), FS_REP, 0, 0)]
    all_to_all x5 -> x1, blocking collectives: 133 us -> 15.1 us  [sum_at_owner(): lax.all_to_all(split_up(value, dim, devices), axis, 0, 0, tiled=True)]
    all_to_all x10 -> x2, blocking collectives: 122 us -> 21.5 us  [from_everyone(): lax.all_to_all(jnp.broadcast_to(value[None], (devices, *value.shape)), ax...]
    all_to_all x6 -> x10, waiting for transfers between devices: 90.6 us -> 179 us  [sum_at_owner(): lax.all_to_all(split_up(value, dim, devices), axis, 0, 0, tiled=True)]
    all_gather x3 -> x0, blocking collectives: 67.1 us -> none  [spread(): return lax.all_gather(share, FS_REP, axis=0, tiled=True)]
    all_to_all x8 -> x16, waiting for transfers between devices: 60.8 us -> 110 us  [from_everyone(): lax.all_to_all(jnp.broadcast_to(value[None], (devices, *value.shape)), ax...]
    all_gather x6 -> x0, waiting for transfers between devices: 37.9 us -> none  [spread(): return lax.all_gather(share, FS_REP, axis=0, tiled=True)]
    all_to_all x0 -> x8, starting transfers between devices: none -> 33.8 us  [spread(): lax.all_to_all(jnp.stack([share] * lax.axis_size(FS_REP)), FS_REP, 0, 0)]
  transfers between devices with their start and end apart: 20 -> 34, of which waited for: 14 -> 33; matrix products, arithmetic and copies ran while one was open for 8% -> 9% of each run, Pallas kernels for 0% -> 0%
where the time goes in v1:
time: 837 us; the launch traced here: 831 us
  waiting for transfers between devices  475 us (57%)
  starting transfers between devices  144 us (17%)
  blocking collectives  82.4 us (10%)
  local copies, waits for them, and re-layouts  53.5 us (6%)
  matrix products  46.4 us (6%)
  other arithmetic  25.2 us (3%)
    all_to_all x8, waiting for transfers between devices, spread(): lax.all_to_all(jnp.stack([share] * lax.axis_size(FS_REP)), FS_REP, 0, 0)  186 us
    all_to_all x10, waiting for transfers between devices, sum_at_owner(): lax.all_to_all(split_up(value, dim, devices), axis, 0, 0, tiled=True)  179 us
    all_to_all x16, waiting for transfers between devices, from_everyone(): lax.all_to_all(jnp.broadcast_to(value[None], (devices, *value.shape)), ax...  110 us
    all_to_all x16, starting transfers between devices, from_everyone(): lax.all_to_all(jnp.broadcast_to(value[None], (devices, *value.shape)), ax...  56.9 us
    all_to_all x10, starting transfers between devices, sum_at_owner(): lax.all_to_all(split_up(value, dim, devices), axis, 0, 0, tiled=True)  53 us
    all_to_all x8, starting transfers between devices, spread(): lax.all_to_all(jnp.stack([share] * lax.axis_size(FS_REP)), FS_REP, 0, 0)  33.8 us
    psum x4, blocking collectives, by_axis(): value = lax.psum(value, axis)  30.8 us
    all_to_all x2, blocking collectives, from_everyone(): lax.all_to_all(jnp.broadcast_to(value[None], (devices, *value.shape)), ax...  21.5 us
  transfers between devices with their start and end apart: 34, of which 33 were waited for; matrix products, arithmetic and copies ran while one was open for 9% of the time, Pallas kernels for 0%

profile of v1, /device:TPU:0, one launch (start us, length us, event | category | flops | bytes accessed | tf_op | source)
XLA Modules:
  0.0 831.5 jit_solution(3619428140870326873)
XLA Ops:
  25.5 13.1 %all_to_all.190 = bf16[4,176,512]{2,1,0:T(8,128)(2,1)S(1)} all-to-all(bf16[4,176,512]{2,1,0:T(8,128)(2,1)S(1)} %broadcast_in_dim.42), channel_id=1, replica_groups=mesh['fs_0'=4,'fs_1'=4,'tp'=4,'rep'=2] {'tp'}, dimensions={0} | all-to-all | bytes 1441792 | tf_op jit(solution)/shard_map/all_to_all | solution.py:31
  44.2 8.4 %all-to-all-done.1 = bf16[4,176,512]{2,1,0:T(8,128)(2,1)S(1)} async-done(((bf16[4,176,512]{2,1,0:T(8,128)(2,1)}), bf16[4,176,512]{2,1,0:T(8,128)(2,1)S(1)}, u32[]{:S(2)}, u32[]{:S(2)}) %all-to-all-start.1) | async-done | bytes 720928 | tf_op jit(solution)/shard_map/all_to_all | solution.py:31
  52.6 8.3 %all-to-all-start.27 = ((bf16[32,32,256]{2,1,0:T(8,128)(2,1)}), bf16[32,32,256]{2,1,0:T(8,128)(2,1)S(1)}, u32[]{:S(2)}, u32[]{:S(2)}) async-start(bf16[32,32,256]{2,1,0:T(8,128)(2,1)} %bitcast.30), calls=%async_computation.27 | async-start | bytes 1048576 | tf_op jit(solution)/shard_map/all_to_all | solution.py:47
  63.2 9.4 %all-to-all-done.27 = bf16[32,32,256]{2,1,0:T(8,128)(2,1)S(1)} async-done(((bf16[32,32,256]{2,1,0:T(8,128)(2,1)}), bf16[32,32,256]{2,1,0:T(8,128)(2,1)S(1)}, u32[]{:S(2)}, u32[]{:S(2)}) %all-to-all-start.27) | async-done | bytes 524320 | tf_op jit(solution)/shard_map/all_to_all | solution.py:47
  81.6 25.9 %all-to-all-done.14 = bf16[32,64,512]{2,1,0:T(8,128)(2,1)S(1)} async-done(((bf16[32,64,512]{2,1,0:T(8,128)(2,1)}), bf16[32,64,512]{2,1,0:T(8,128)(2,1)S(1)}, u32[]{:S(2)}, u32[]{:S(2)}) %all-to-all-start.14) | async-done | bytes 2097184 | tf_op jit(solution)/shard_map/all_to_all | solution.py:47
  116.2 26.1 %all-to-all-done.2 = bf16[32,64,512]{2,1,0:T(8,128)(2,1)} async-done(((bf16[32,64,512]{2,1,0:T(8,128)(2,1)}), bf16[32,64,512]{2,1,0:T(8,128)(2,1)}, u32[]{:S(2)}, u32[]{:S(2)}) %all-to-all-start.2) | async-done | bytes 2097184 | tf_op jit(solution)/shard_map/all_to_all | solution.py:47
  145.5 8.4 %all-reduce.2 = (f32[]{:T(128)}, f32[]{:T(128)}, f32[]{:T(128)}, f32[]{:T(128)}, f32[]{:T(128)}, /*index=5*/f32[]{:T(128)}) all-reduce(f32[]{:T(128)} %multiply_reduce_fusion.1, f32[]{:T(128)} %get-tuple-element.39, f32[]{:T(128)} %multiply_reduce_fusion, ...), channel_id=1, replica_groups=mesh['fs_0'=4,'fs_1'=4,'tp'=4,'rep'=2] {'fs_0'}, use_global_device_ids=true, to_apply=%region_3.0 | all-reduce | flops 6 | bytes 48 | tf_op jit(solution)/shard_map/psum | solution.py:53
  153.9 9.6 %all-reduce.1 = (f32[]{:T(128)}, f32[]{:T(128)}, f32[]{:T(128)}, f32[]{:T(128)}, f32[]{:T(128)}, /*index=5*/f32[]{:T(128)}) all-reduce(f32[]{:T(128)} %get-tuple-element.18, f32[]{:T(128)} %get-tuple-element.19, f32[]{:T(128)} %get-tuple-element.20, f32[]{:T(128)} %get-tuple-element.21, ...), channel_id=1, replica_groups=mesh['fs_0'=4,'fs_1'=4,'tp'=4,'rep'=2] {'fs_1'}, use_global_device_ids=true, to_apply=%region_4.0 | all-reduce | flops 6 | bytes 48 | tf_op jit(solution)/shard_map/psum | solution.py:53
  163.5 9.6 %all-reduce = (f32[]{:T(128)}, f32[]{:T(128)}, f32[]{:T(128)}, f32[]{:T(128)}, f32[]{:T(128)}, /*index=5*/f32[]{:T(128)}) all-reduce(f32[]{:T(128)} %get-tuple-element.12, f32[]{:T(128)} %get-tuple-element.13, f32[]{:T(128)} %get-tuple-element.14, f32[]{:T(128)} %get-tuple-element.15, ...), channel_id=1, replica_groups=mesh['fs_0'=4,'fs_1'=4,'tp'=4,'rep'=2] {'tp'}, use_global_device_ids=true, to_apply=%region_5.0 | all-reduce | flops 6 | bytes 48 | tf_op jit(solution)/shard_map/psum | solution.py:53
  182.5 11.6 %all-to-all-done.28 = bf16[32,32,256]{2,1,0:T(8,128)(2,1)S(1)} async-done(((bf16[32,32,256]{2,1,0:T(8,128)(2,1)}), bf16[32,32,256]{2,1,0:T(8,128)(2,1)S(1)}, u32[]{:S(2)}, u32[]{:S(2)}) %all-to-all-start.28) | async-done | bytes 524320 | tf_op jit(solution)/shard_map/all_to_all | solution.py:82
  204.5 8.4 %all_to_all.191 = bf16[4,64,256]{2,1,0:T(8,128)(2,1)S(1)} all-to-all(bf16[4,64,256]{2,1,0:T(8,128)(2,1)S(1)} %broadcast_in_dim.50), channel_id=1, replica_groups=mesh['fs_0'=4,'fs_1'=4,'tp'=4,'rep'=2] {'tp'}, dimensions={0} | all-to-all | bytes 262144 | tf_op jit(solution)/shard_map/all_to_all | solution.py:31
  213.2 15.1 %all_to_all.192 = bf16[32,32,256]{2,1,0:T(8,128)(2,1)S(1)} all-to-all(bf16[32,32,256]{2,1,0:T(8,128)(2,1)S(1)} %bitcast.187), channel_id=1, replica_groups=mesh['fs_0'=4,'fs_1'=4,'tp'=4,'rep'=2] {'fs_0','fs_1','rep'}, dimensions={0} | all-to-all | bytes 1048576 | tf_op jit(solution)/shard_map/all_to_all | solution.py:47
  228.4 15.1 %all_to_all.193 = bf16[32,32,256]{2,1,0:T(8,128)(2,1)S(1)} all-to-all(bf16[32,32,256]{2,1,0:T(8,128)(2,1)S(1)} %stack.25), channel_id=1, replica_groups=mesh['fs_0'=4,'fs_1'=4,'tp'=4,'rep'=2] {'fs_0','fs_1','rep'}, dimensions={0} | all-to-all | bytes 1048576 | tf_op jit(solution)/shard_map/all_to_all | solution.py:82
  272.3 27.3 %all-to-all-done.15 = bf16[32,64,512]{2,1,0:T(8,128)(2,1)S(1)} async-done(((bf16[32,64,512]{2,1,0:T(8,128)(2,1)}), bf16[32,64,512]{2,1,0:T(8,128)(2,1)S(1)}, u32[]{:S(2)}, u32[]{:S(2)}) %all-to-all-start.15) | async-done | bytes 2097184 | tf_op jit(solution)/shard_map/all_to_all | solution.py:82
  310.2 26.6 %all-to-all-done.3 = bf16[32,64,512]{2,1,0:T(8,128)(2,1)} async-done(((bf16[32,64,512]{2,1,0:T(8,128)(2,1)}), bf16[32,64,512]{2,1,0:T(8,128)(2,1)}, u32[]{:S(2)}, u32[]{:S(2)}) %all-to-all-start.3) | async-done | bytes 2097184 | tf_op jit(solution)/shard_map/all_to_all | solution.py:82
  342.7 10.3 %all-to-all-done.35 = bf16[32,32,256]{2,1,0:T(8,128)(2,1)} async-done(((bf16[32,32,256]{2,1,0:T(8,128)(2,1)}), bf16[32,32,256]{2,1,0:T(8,128)(2,1)}, u32[]{:S(2)}, u32[]{:S(2)}) %all-to-all-start.35) | async-done | bytes 524320 | tf_op jit(solution)/shard_map/all_to_all | solution.py:47
  359.4 11.0 %all-to-all-done.16 = bf16[4,176,512]{2,1,0:T(8,128)(2,1)S(1)} async-done(((bf16[4,176,512]{2,1,0:T(8,128)(2,1)}), bf16[4,176,512]{2,1,0:T(8,128)(2,1)S(1)}, u32[]{:S(2)}, u32[]{:S(2)}) %all-to-all-start.16) | async-done | bytes 720928 | tf_op jit(solution)/shard_map/all_to_all | solution.py:31
  377.7 9.2 %all-to-all-done.36 = bf16[32,32,256]{2,1,0:T(8,128)(2,1)S(1)} async-done(((bf16[32,32,256]{2,1,0:T(8,128)(2,1)}), bf16[32,32,256]{2,1,0:T(8,128)(2,1)S(1)}, u32[]{:S(2)}, u32[]{:S(2)}) %all-to-all-start.36) | async-done | bytes 524320 | tf_op jit(solution)/shard_map/all_to_all | solution.py:82
  394.8 8.9 %all-to-all-done.4 = bf16[4,176,512]{2,1,0:T(8,128)(2,1)S(1)} async-done(((bf16[4,176,512]{2,1,0:T(8,128)(2,1)}), bf16[4,176,512]{2,1,0:T(8,128)(2,1)S(1)}, u32[]{:S(2)}, u32[]{:S(2)}) %all-to-all-start.4) | async-done | bytes 720928 | tf_op jit(solution)/shard_map/all_to_all | solution.py:31
  420.3 7.8 all-to-all-done.17
  452.1 25.8 %all-to-all-done.18 = bf16[32,64,512]{2,1,0:T(8,128)(2,1)S(1)} async-done(((bf16[32,64,512]{2,1,0:T(8,128)(2,1)}), bf16[32,64,512]{2,1,0:T(8,128)(2,1)S(1)}, u32[]{:S(2)}, u32[]{:S(2)}) %all-to-all-start.18) | async-done | bytes 2097184 | tf_op jit(solution)/shard_map/all_to_all | solution.py:47
  485.9 27.6 %all-to-all-done.6 = bf16[32,64,512]{2,1,0:T(8,128)(2,1)S(1)} async-done(((bf16[32,64,512]{2,1,0:T(8,128)(2,1)}), bf16[32,64,512]{2,1,0:T(8,128)(2,1)S(1)}, u32[]{:S(2)}, u32[]{:S(2)}) %all-to-all-start.6) | async-done | bytes 2097184 | tf_op jit(solution)/shard_map/all_to_all | solution.py:47
  522.5 27.6 %all-to-all-done.19 = bf16[32,64,512]{2,1,0:T(8,128)(2,1)S(1)} async-done(((bf16[32,64,512]{2,1,0:T(8,128)(2,1)}), bf16[32,64,512]{2,1,0:T(8,128)(2,1)S(1)}, u32[]{:S(2)}, u32[]{:S(2)}) %all-to-all-start.19) | async-done | bytes 2097184 | tf_op jit(solution)/shard_map/all_to_all | solution.py:82
  559.4 27.3 %all-to-all-done.7 = bf16[32,64,512]{2,1,0:T(8,128)(2,1)S(1)} async-done(((bf16[32,64,512]{2,1,0:T(8,128)(2,1)}), bf16[32,64,512]{2,1,0:T(8,128)(2,1)S(1)}, u32[]{:S(2)}, u32[]{:S(2)}) %all-to-all-start.7) | async-done | bytes 2097184 | tf_op jit(solution)/shard_map/all_to_all | solution.py:82
  593.2 9.1 %all-to-all-done.20 = bf16[4,176,512]{2,1,0:T(8,128)(2,1)S(1)} async-done(((bf16[4,176,512]{2,1,0:T(8,128)(2,1)}), bf16[4,176,512]{2,1,0:T(8,128)(2,1)S(1)}, u32[]{:S(2)}, u32[]{:S(2)}) %all-to-all-start.20) | async-done | bytes 720928 | tf_op jit(solution)/shard_map/all_to_all | solution.py:31
  623.2 7.4 all-to-all-done.21
  645.0 11.0 %all-to-all-start.22 = ((bf16[32,64,512]{2,1,0:T(8,128)(2,1)}), bf16[32,64,512]{2,1,0:T(8,128)(2,1)S(1)}, u32[]{:S(2)}, u32[]{:S(2)}) async-start(bf16[32,64,512]{2,1,0:T(8,128)(2,1)} %bitcast.151), calls=%async_computation.22 | async-start | bytes 4194304 | tf_op jit(solution)/shard_map/all_to_all | solution.py:47
  660.2 25.8 %all-to-all-done.22 = bf16[32,64,512]{2,1,0:T(8,128)(2,1)S(1)} async-done(((bf16[32,64,512]{2,1,0:T(8,128)(2,1)}), bf16[32,64,512]{2,1,0:T(8,128)(2,1)S(1)}, u32[]{:S(2)}, u32[]{:S(2)}) %all-to-all-start.22) | async-done | bytes 2097184 | tf_op jit(solution)/shard_map/all_to_all | solution.py:47
  694.0 27.6 %all-to-all-done.10 = bf16[32,64,512]{2,1,0:T(8,128)(2,1)S(1)} async-done(((bf16[32,64,512]{2,1,0:T(8,128)(2,1)}), bf16[32,64,512]{2,1,0:T(8,128)(2,1)S(1)}, u32[]{:S(2)}, u32[]{:S(2)}) %all-to-all-start.10) | async-done | bytes 2097184 | tf_op jit(solution)/shard_map/all_to_all | solution.py:47
  730.8 27.6 %all-to-all-done.23 = bf16[32,64,512]{2,1,0:T(8,128)(2,1)S(1)} async-done(((bf16[32,64,512]{2,1,0:T(8,128)(2,1)}), bf16[32,64,512]{2,1,0:T(8,128)(2,1)S(1)}, u32[]{:S(2)}, u32[]{:S(2)}) %all-to-all-start.23) | async-done | bytes 2097184 | tf_op jit(solution)/shard_map/all_to_all | solution.py:82
  766.8 28.9 %all-to-all-done.11 = bf16[32,64,512]{2,1,0:T(8,128)(2,1)} async-done(((bf16[32,64,512]{2,1,0:T(8,128)(2,1)}), bf16[32,64,512]{2,1,0:T(8,128)(2,1)}, u32[]{:S(2)}, u32[]{:S(2)}) %all-to-all-start.11) | async-done | bytes 2097184 | tf_op jit(solution)/shard_map/all_to_all | solution.py:82
  803.9 8.2 all-to-all-done.24
  (240 shorter events, 302.2 us)
Async XLA Ops:
  15.0 10.4 %all-to-all-start.26 = ((bf16[4,64,256]{2,1,0:T(8,128)(2,1)}), bf16[4,64,256]{2,1,0:T(8,128)(2,1)S(1)}, u32[]{:S(2)}, u32[]{:S(2)}) async-start(bf16[4,64,256]{2,1,0:T(8,128)(2,1)} %broadcast_in_dim.48), calls=%async_computation.26 | async-start | bytes 262144 | tf_op jit(solution)/shard_map/all_to_all | solution.py:31
  39.5 13.0 %all-to-all-start.1 = ((bf16[4,176,512]{2,1,0:T(8,128)(2,1)}), bf16[4,176,512]{2,1,0:T(8,128)(2,1)S(1)}, u32[]{:S(2)}, u32[]{:S(2)}) async-start(bf16[4,176,512]{2,1,0:T(8,128)(2,1)} %broadcast_in_dim.36), calls=%async_computation.1 | async-start | bytes 1441792 | tf_op jit(solution)/shard_map/all_to_all | solution.py:31
  52.6 19.9 %all-to-all-start.27 = ((bf16[32,32,256]{2,1,0:T(8,128)(2,1)}), bf16[32,32,256]{2,1,0:T(8,128)(2,1)S(1)}, u32[]{:S(2)}, u32[]{:S(2)}) async-start(bf16[32,32,256]{2,1,0:T(8,128)(2,1)} %bitcast.30), calls=%async_computation.27 | async-start | bytes 1048576 | tf_op jit(solution)/shard_map/all_to_all | solution.py:47
  73.3 34.1 %all-to-all-start.14 = ((bf16[32,64,512]{2,1,0:T(8,128)(2,1)}), bf16[32,64,512]{2,1,0:T(8,128)(2,1)S(1)}, u32[]{:S(2)}, u32[]{:S(2)}) async-start(bf16[32,64,512]{2,1,0:T(8,128)(2,1)} %bitcast.149), calls=%async_computation.14 | async-start | bytes 4194304 | tf_op jit(solution)/shard_map/all_to_all | solution.py:47
  107.5 34.8 %all-to-all-start.2 = ((bf16[32,64,512]{2,1,0:T(8,128)(2,1)}), bf16[32,64,512]{2,1,0:T(8,128)(2,1)}, u32[]{:S(2)}, u32[]{:S(2)}) async-start(bf16[32,64,512]{2,1,0:T(8,128)(2,1)} %bitcast.148), calls=%async_computation.2 | async-start | bytes 4194304 | tf_op jit(solution)/shard_map/all_to_all | solution.py:47
  178.5 15.6 %all-to-all-start.28 = ((bf16[32,32,256]{2,1,0:T(8,128)(2,1)}), bf16[32,32,256]{2,1,0:T(8,128)(2,1)S(1)}, u32[]{:S(2)}, u32[]{:S(2)}) async-start(bf16[32,32,256]{2,1,0:T(8,128)(2,1)} %stack.24), calls=%async_computation.28 | async-start | bytes 1048576 | tf_op jit(solution)/shard_map/all_to_all | solution.py:82
  195.0 9.3 %all-to-all-start.29 = ((bf16[4,64,256]{2,1,0:T(8,128)(2,1)}), bf16[4,64,256]{2,1,0:T(8,128)(2,1)S(1)}, u32[]{:S(2)}, u32[]{:S(2)}) async-start(bf16[4,64,256]{2,1,0:T(8,128)(2,1)} %broadcast_in_dim.49), calls=%async_computation.29 | async-start | bytes 262144 | tf_op jit(solution)/shard_map/all_to_all | solution.py:31
  244.3 9.3 %all-to-all-start.33 = ((bf16[4,64,256]{2,1,0:T(8,128)(2,1)}), bf16[4,64,256]{2,1,0:T(8,128)(2,1)S(1)}, u32[]{:S(2)}, u32[]{:S(2)}) async-start(bf16[4,64,256]{2,1,0:T(8,128)(2,1)} %broadcast_in_dim.51), calls=%async_computation.33 | async-start | bytes 262144 | tf_op jit(solution)/shard_map/all_to_all | solution.py:31
  254.5 9.3 %all-to-all-start.34 = ((bf16[4,64,256]{2,1,0:T(8,128)(2,1)}), bf16[4,64,256]{2,1,0:T(8,128)(2,1)S(1)}, u32[]{:S(2)}, u32[]{:S(2)}) async-start(bf16[4,64,256]{2,1,0:T(8,128)(2,1)} %broadcast_in_dim.52), calls=%async_computation.34 | async-start | bytes 262144 | tf_op jit(solution)/shard_map/all_to_all | solution.py:31
  265.4 34.1 %all-to-all-start.15 = ((bf16[32,64,512]{2,1,0:T(8,128)(2,1)}), bf16[32,64,512]{2,1,0:T(8,128)(2,1)S(1)}, u32[]{:S(2)}, u32[]{:S(2)}) async-start(bf16[32,64,512]{2,1,0:T(8,128)(2,1)} %stack.21), calls=%async_computation.15 | async-start | bytes 4194304 | tf_op jit(solution)/shard_map/all_to_all | solution.py:82
  301.9 34.8 %all-to-all-start.3 = ((bf16[32,64,512]{2,1,0:T(8,128)(2,1)}), bf16[32,64,512]{2,1,0:T(8,128)(2,1)}, u32[]{:S(2)}, u32[]{:S(2)}) async-start(bf16[32,64,512]{2,1,0:T(8,128)(2,1)} %stack.18), calls=%async_computation.3 | async-start | bytes 4194304 | tf_op jit(solution)/shard_map/all_to_all | solution.py:82
  336.8 16.2 %all-to-all-start.35 = ((bf16[32,32,256]{2,1,0:T(8,128)(2,1)}), bf16[32,32,256]{2,1,0:T(8,128)(2,1)}, u32[]{:S(2)}, u32[]{:S(2)}) async-start(bf16[32,32,256]{2,1,0:T(8,128)(2,1)} %bitcast.186), calls=%async_computation.35 | async-start | bytes 1048576 | tf_op jit(solution)/shard_map/all_to_all | solution.py:47
  354.8 15.6 %all-to-all-start.16 = ((bf16[4,176,512]{2,1,0:T(8,128)(2,1)}), bf16[4,176,512]{2,1,0:T(8,128)(2,1)S(1)}, u32[]{:S(2)}, u32[]{:S(2)}) async-start(bf16[4,176,512]{2,1,0:T(8,128)(2,1)} %broadcast_in_dim.43), calls=%async_computation.16 | async-start | bytes 1441792 | tf_op jit(solution)/shard_map/all_to_all | solution.py:31
  371.5 15.5 %all-to-all-start.36 = ((bf16[32,32,256]{2,1,0:T(8,128)(2,1)}), bf16[32,32,256]{2,1,0:T(8,128)(2,1)S(1)}, u32[]{:S(2)}, u32[]{:S(2)}) async-start(bf16[32,32,256]{2,1,0:T(8,128)(2,1)} %stack.26), calls=%async_computation.36 | async-start | bytes 1048576 | tf_op jit(solution)/shard_map/all_to_all | solution.py:82
  388.0 15.7 %all-to-all-start.4 = ((bf16[4,176,512]{2,1,0:T(8,128)(2,1)}), bf16[4,176,512]{2,1,0:T(8,128)(2,1)S(1)}, u32[]{:S(2)}, u32[]{:S(2)}) async-start(bf16[4,176,512]{2,1,0:T(8,128)(2,1)} %broadcast_in_dim.37), calls=%async_computation.4 | async-start | bytes 1441792 | tf_op jit(solution)/shard_map/all_to_all | solution.py:31
  404.4 9.3 %all-to-all-start.37 = ((bf16[4,64,256]{2,1,0:T(8,128)(2,1)}), bf16[4,64,256]{2,1,0:T(8,128)(2,1)S(1)}, u32[]{:S(2)}, u32[]{:S(2)}) async-start(bf16[4,64,256]{2,1,0:T(8,128)(2,1)} %broadcast_in_dim.53), calls=%async_computation.37 | async-start | bytes 262144 | tf_op jit(solution)/shard_map/all_to_all | solution.py:31
  414.6 13.6 %all-to-all-start.17 = ((bf16[4,176,512]{2,1,0:T(8,128)(2,1)}), bf16[4,176,512]{2,1,0:T(8,128)(2,1)S(1)}, u32[]{:S(2)}, u32[]{:S(2)}) async-start(bf16[4,176,512]{2,1,0:T(8,128)(2,1)} %broadcast_in_dim.44), calls=%async_computation.17 | async-start | bytes 1441792 | tf_op jit(solution)/shard_map/all_to_all | solution.py:31
  429.1 12.6 %all-to-all-start.5 = ((bf16[4,176,512]{2,1,0:T(8,128)(2,1)}), bf16[4,176,512]{2,1,0:T(8,128)(2,1)S(1)}, u32[]{:S(2)}, u32[]{:S(2)}) async-start(bf16[4,176,512]{2,1,0:T(8,128)(2,1)} %broadcast_in_dim.38), calls=%async_computation.5 | async-start | bytes 1441792 | tf_op jit(solution)/shard_map/all_to_all | solution.py:31
  442.5 35.4 %all-to-all-start.18 = ((bf16[32,64,512]{2,1,0:T(8,128)(2,1)}), bf16[32,64,512]{2,1,0:T(8,128)(2,1)S(1)}, u32[]{:S(2)}, u32[]{:S(2)}) async-start(bf16[32,64,512]{2,1,0:T(8,128)(2,1)} %bitcast.150), calls=%async_computation.18 | async-start | bytes 4194304 | tf_op jit(solution)/shard_map/all_to_all | solution.py:47
  479.3 34.1 %all-to-all-start.6 = ((bf16[32,64,512]{2,1,0:T(8,128)(2,1)}), bf16[32,64,512]{2,1,0:T(8,128)(2,1)S(1)}, u32[]{:S(2)}, u32[]{:S(2)}) async-start(bf16[32,64,512]{2,1,0:T(8,128)(2,1)} %bitcast.152), calls=%async_computation.6 | async-start | bytes 4194304 | tf_op jit(solution)/shard_map/all_to_all | solution.py:47
  515.9 34.1 %all-to-all-start.19 = ((bf16[32,64,512]{2,1,0:T(8,128)(2,1)}), bf16[32,64,512]{2,1,0:T(8,128)(2,1)S(1)}, u32[]{:S(2)}, u32[]{:S(2)}) async-start(bf16[32,64,512]{2,1,0:T(8,128)(2,1)} %stack.22), calls=%async_computation.19 | async-start | bytes 4194304 | tf_op jit(solution)/shard_map/all_to_all | solution.py:82
  552.5 34.1 %all-to-all-start.7 = ((bf16[32,64,512]{2,1,0:T(8,128)(2,1)}), bf16[32,64,512]{2,1,0:T(8,128)(2,1)S(1)}, u32[]{:S(2)}, u32[]{:S(2)}) async-start(bf16[32,64,512]{2,1,0:T(8,128)(2,1)} %stack.19), calls=%async_computation.7 | async-start | bytes 4194304 | tf_op jit(solution)/shard_map/all_to_all | solution.py:82
  588.5 13.9 %all-to-all-start.20 = ((bf16[4,176,512]{2,1,0:T(8,128)(2,1)}), bf16[4,176,512]{2,1,0:T(8,128)(2,1)S(1)}, u32[]{:S(2)}, u32[]{:S(2)}) async-start(bf16[4,176,512]{2,1,0:T(8,128)(2,1)} %broadcast_in_dim.45), calls=%async_computation.20 | async-start | bytes 1441792 | tf_op jit(solution)/shard_map/all_to_all | solution.py:31
  604.4 12.7 %all-to-all-start.8 = ((bf16[4,176,512]{2,1,0:T(8,128)(2,1)}), bf16[4,176,512]{2,1,0:T(8,128)(2,1)S(1)}, u32[]{:S(2)}, u32[]{:S(2)}) async-start(bf16[4,176,512]{2,1,0:T(8,128)(2,1)} %broadcast_in_dim.39), calls=%async_computation.8 | async-start | bytes 1441792 | tf_op jit(solution)/shard_map/all_to_all | solution.py:31
  618.0 12.6 %all-to-all-start.21 = ((bf16[4,176,512]{2,1,0:T(8,128)(2,1)}), bf16[4,176,512]{2,1,0:T(8,128)(2,1)S(1)}, u32[]{:S(2)}, u32[]{:S(2)}) async-start(bf16[4,176,512]{2,1,0:T(8,128)(2,1)} %broadcast_in_dim.46), calls=%async_computation.21 | async-start | bytes 1441792 | tf_op jit(solution)/shard_map/all_to_all | solution.py:31
  631.6 12.6 %all-to-all-start.9 = ((bf16[4,176,512]{2,1,0:T(8,128)(2,1)}), bf16[4,176,512]{2,1,0:T(8,128)(2,1)S(1)}, u32[]{:S(2)}, u32[]{:S(2)}) async-start(bf16[4,176,512]{2,1,0:T(8,128)(2,1)} %broadcast_in_dim.40), calls=%async_computation.9 | async-start | bytes 1441792 | tf_op jit(solution)/shard_map/all_to_all | solution.py:31
  645.0 41.0 %all-to-all-start.22 = ((bf16[32,64,512]{2,1,0:T(8,128)(2,1)}), bf16[32,64,512]{2,1,0:T(8,128)(2,1)S(1)}, u32[]{:S(2)}, u32[]{:S(2)}) async-start(bf16[32,64,512]{2,1,0:T(8,128)(2,1)} %bitcast.151), calls=%async_computation.22 | async-start | bytes 4194304 | tf_op jit(solution)/shard_map/all_to_all | solution.py:47
  687.4 34.1 %all-to-all-start.10 = ((bf16[32,64,512]{2,1,0:T(8,128)(2,1)}), bf16[32,64,512]{2,1,0:T(8,128)(2,1)S(1)}, u32[]{:S(2)}, u32[]{:S(2)}) async-start(bf16[32,64,512]{2,1,0:T(8,128)(2,1)} %bitcast.153), calls=%async_computation.10 | async-start | bytes 4194304 | tf_op jit(solution)/shard_map/all_to_all | solution.py:47
  724.0 34.3 %all-to-all-start.23 = ((bf16[32,64,512]{2,1,0:T(8,128)(2,1)}), bf16[32,64,512]{2,1,0:T(8,128)(2,1)S(1)}, u32[]{:S(2)}, u32[]{:S(2)}) async-start(bf16[32,64,512]{2,1,0:T(8,128)(2,1)} %stack.23), calls=%async_computation.23 | async-start | bytes 4194304 | tf_op jit(solution)/shard_map/all_to_all | solution.py:82
  760.8 34.8 %all-to-all-start.11 = ((bf16[32,64,512]{2,1,0:T(8,128)(2,1)}), bf16[32,64,512]{2,1,0:T(8,128)(2,1)}, u32[]{:S(2)}, u32[]{:S(2)}) async-start(bf16[32,64,512]{2,1,0:T(8,128)(2,1)} %stack.20), calls=%async_computation.11 | async-start | bytes 4194304 | tf_op jit(solution)/shard_map/all_to_all | solution.py:82
  797.5 14.6 %all-to-all-start.24 = ((bf16[4,176,512]{2,1,0:T(8,128)(2,1)}), bf16[4,176,512]{2,1,0:T(8,128)(2,1)}, u32[]{:S(2)}, u32[]{:S(2)}) async-start(bf16[4,176,512]{2,1,0:T(8,128)(2,1)} %broadcast_in_dim.47), calls=%async_computation.24 | async-start | bytes 1441792 | tf_op jit(solution)/shard_map/all_to_all | solution.py:31
  813.0 12.7 %all-to-all-start.12 = ((bf16[4,176,512]{2,1,0:T(8,128)(2,1)}), bf16[4,176,512]{2,1,0:T(8,128)(2,1)S(1)}, u32[]{:S(2)}, u32[]{:S(2)}) async-start(bf16[4,176,512]{2,1,0:T(8,128)(2,1)} %broadcast_in_dim.41), calls=%async_computation.12 | async-start | bytes 1441792 | tf_op jit(solution)/shard_map/all_to_all | solution.py:31
  (52 other events, 635.9 us)
